TPU v7x, 32 devices: a whole 2x2x4 slice. The times are simulated.
32 devices in a mesh: kv: 8 (over z, y), tp: 4 (over x, core).
Axes of the slice: x: 2, y: 2, z: 4, core: 2. Of those that a mesh axis runs over, the one named last changes fastest.
Arguments:
- hidden: bfloat16 [128, 4096], P(None, 'tp'), may hold values from -50 to 50
- input_gain: bfloat16 [4096], P('tp'), may hold values from 0.099609375 to 1.8984375
- x_weight: bfloat16 [4096, 8192], P('tp', 'kv'), may hold values from -0.09375 to 0.09375
- z_weight: bfloat16 [4096, 8192], P('tp', 'kv'), may hold values from -0.09375 to 0.09375
- bc_weight: bfloat16 [4096, 8192], P('tp', 'kv'), may hold values from -0.09375 to 0.09375
- dt_weight: bfloat16 [4096, 128], P('tp', 'kv'), may hold values from -0.09375 to 0.09375
- x_kernel: bfloat16 [4, 8192], P(None, 'kv'), may hold values from -3 to 3
- bc_kernel: bfloat16 [4, 8192], P(None, 'kv'), may hold values from -3 to 3
- dt_bias: float32 [128], P('kv'), may hold values from -3 to 0.5
- decay_log: float32 [128], P('kv'), may hold values from -3 to 1.5
- skip_scale: float32 [128], P('kv'), may hold values from 0.5 to 1.5
- output_gain: bfloat16 [8192], P('kv'), may hold values from 0.099609375 to 1.8984375
- output_weight: bfloat16 [8192, 4096], P('kv'), may hold values from -0.09375 to 0.09375
- saved_states: float32 [32, 5, 128, 64, 128], P('tp', None, 'kv'), may hold values from -1.8 to 1.8
- x_history: bfloat16 [32, 7, 8192], P('tp', None, 'kv'), may hold values from -6 to 6
- bc_history: bfloat16 [32, 7, 8192], P('tp', None, 'kv'), may hold values from -6 to 6
- accepted: int32 [32], P('tp'), may hold values from 0 to 4
Outputs:
- mixed: bfloat16 [128, 4096], P('tp', 'kv')
- new_states: float32 [32, 5, 128, 64, 128], P('tp', None, 'kv')
- x_window: bfloat16 [32, 7, 8192], P('tp', None, 'kv')
- bc_window: bfloat16 [32, 7, 8192], P('tp', None, 'kv')
All inputs are finite; a program needn't handle non-finite values.
Results may differ from a plain program's by a relative error of at most 0.02.
Values may be sent and summed in bfloat16 or wider, within the bound.
A program may use at most 192 MiB of HBM per device.

v0:
```python
import jax
import jax.numpy as jnp
from jax import lax
from jax.sharding import PartitionSpec as P

D = 4096
PROPS = 4
INNER = 8192
EPSILON = 1e-05


def partner_2(block, axis, stride):
    count = lax.axis_size(axis)
    route = []
    for low in range(count):
        high = low | 1 << stride
        if high != low and high < count:
            route += [(low, high), (high, low)]
    return lax.ppermute(block, axis, route)


def take_window(history, accepted, fresh_rows):
    history_len = history.shape[1] - fresh_rows.shape[1]
    indices = accepted[:, None] + jnp.arange(history_len, dtype=jnp.int32)[None, :]
    kept_rows = jnp.take_along_axis(history, indices[:, :, None], axis=1)
    return jnp.concatenate([kept_rows, fresh_rows], axis=1)


def conv_silu(window, kernel):
    length = window.shape[1] - kernel.shape[0] + 1
    running = window[:, 0:length].astype(jnp.float32) * kernel[0].astype(jnp.float32)
    for offset in range(1, kernel.shape[0]):
        running = running + window[:, offset : offset + length].astype(jnp.float32) * kernel[
            offset
        ].astype(jnp.float32)
    return jax.nn.silu(running)


def ssd_block(x_conv, step_size, decay_rate, b_terms, c_terms, first_state, skip_scale):
    cumulated = jnp.cumsum(-decay_rate * step_size, axis=1)
    length = x_conv.shape[1]
    indices = jnp.arange(length)
    causal = indices[:, None] >= indices[None, :]
    gaps = cumulated[:, :, None, :] - cumulated[:, None, :, :]
    weights = jnp.exp(jnp.where(causal[None, :, :, None], gaps, -jnp.inf))
    inputs = x_conv * step_size[..., None]
    outer_prod = jnp.einsum("srhp,srhn->srhpn", inputs, b_terms)
    states = jnp.exp(cumulated)[..., None, None] * first_state[:, None] + jnp.einsum(
        "strh,srhpn->sthpn", weights, outer_prod
    )
    output = jnp.einsum("sthn,sthpn->sthp", c_terms, states) + skip_scale[:, None] * x_conv
    return (output, states)


def local(
    hidden,
    input_gain,
    x_weight,
    z_weight,
    bc_weight,
    dt_weight,
    x_kernel,
    bc_kernel,
    dt_bias,
    decay_log,
    skip_scale,
    output_gain,
    output_weight,
    saved_states,
    x_history,
    bc_history,
    accepted,
):
    heads_here = dt_bias.shape[0]
    head_size = x_weight.shape[1] // heads_here
    state_size = saved_states.shape[4]
    seqs_here = accepted.shape[0]
    rows_here = hidden.shape[0] // lax.axis_size("tp")
    inner_here = x_weight.shape[1]
    bc_here = bc_weight.shape[1]
    widened = hidden.astype(jnp.float32)
    squares = lax.psum(jnp.sum(widened * widened, axis=1), "tp")
    normed = (
        widened * lax.rsqrt(squares[:, None] / D + EPSILON) * input_gain.astype(jnp.float32)
    ).astype(jnp.bfloat16)
    weights = jnp.concatenate([x_weight, z_weight, bc_weight, dt_weight], axis=1)
    product = jnp.dot(normed, weights, preferred_element_type=jnp.float32)
    projected = lax.psum_scatter(
        lax.optimization_barrier(product.astype(jnp.bfloat16))
        .astype(jnp.float32)
        .astype(jnp.bfloat16),
        "tp",
        scatter_dimension=0,
        tiled=True,
    )
    x_fresh = projected[:, :inner_here]
    z_fresh = projected[:, inner_here : 2 * inner_here]
    bc_fresh = projected[:, 2 * inner_here : 2 * inner_here + bc_here]
    dt_fresh = projected[:, 2 * inner_here + bc_here :]
    x_window = take_window(x_history, accepted, x_fresh.reshape(seqs_here, PROPS, inner_here))
    bc_window = take_window(bc_history, accepted, bc_fresh.reshape(seqs_here, PROPS, bc_here))
    x_conv = conv_silu(x_window, x_kernel).reshape(seqs_here, PROPS, heads_here, head_size)
    bc_conv = conv_silu(bc_window, bc_kernel)
    spread = max(4 // heads_here, 1)
    position = lax.axis_index("kv")
    for level in range(spread.bit_length() - 1):
        partner = partner_2(bc_conv, "kv", level)
        low_half = position // 2**level % 2 == 0
        bc_conv = jnp.where(
            low_half,
            jnp.concatenate([bc_conv, partner], axis=2),
            jnp.concatenate([partner, bc_conv], axis=2),
        )
    groups_here = bc_conv.shape[2] // (2 * state_size)
    paired = bc_conv.reshape(seqs_here, PROPS, groups_here, 2, state_size)
    per_group = heads_here // groups_here
    b_terms = jnp.repeat(paired[:, :, :, 0], per_group, axis=2)
    c_terms = jnp.repeat(paired[:, :, :, 1], per_group, axis=2)
    step_size = jax.nn.softplus(
        dt_fresh.astype(jnp.float32).reshape(seqs_here, PROPS, heads_here) + dt_bias
    )
    first_state = jnp.take_along_axis(saved_states, accepted[:, None, None, None, None], axis=1)[
        :, 0
    ]
    output, states = ssd_block(
        x_conv, step_size, jnp.exp(decay_log), b_terms, c_terms, first_state, skip_scale
    )
    new_states = jnp.concatenate([first_state[:, None], states], axis=1)
    gate_values = z_fresh.astype(jnp.float32).reshape(seqs_here, PROPS, heads_here, head_size)
    gated = (output * jax.nn.silu(gate_values)).reshape(rows_here, inner_here)
    square_sum = jnp.sum(gated * gated, axis=1)
    scaled = (gated * output_gain.astype(jnp.float32)).astype(jnp.bfloat16)
    partial_value = jnp.dot(scaled, output_weight, preferred_element_type=jnp.float32)
    total_squares = lax.psum(square_sum, "kv")
    summed = lax.psum_scatter(partial_value, "kv", scatter_dimension=1, tiled=True)
    mixed = (lax.rsqrt(total_squares / INNER + EPSILON)[:, None] * summed).astype(jnp.bfloat16)
    return (mixed, new_states, x_window, bc_window)


def solution(mesh):
    in_specs = (
        P(None, "tp"),
        P("tp"),
        P("tp", "kv"),
        P("tp", "kv"),
        P("tp", "kv"),
        P("tp", "kv"),
        P(None, "kv"),
        P(None, "kv"),
        P("kv"),
        P("kv"),
        P("kv"),
        P("kv"),
        P("kv", None),
        P("tp", None, "kv", None, None),
        P("tp", None, "kv"),
        P("tp", None, "kv"),
        P("tp"),
    )
    out_specs = (
        P("tp", "kv"),
        P("tp", None, "kv", None, None),
        P("tp", None, "kv"),
        P("tp", None, "kv"),
    )
    return jax.shard_map(local, mesh=mesh, in_specs=in_specs, out_specs=out_specs, check_vma=False)
```

profile of v0, /device:TPU:0, one launch (start us, length us, event | category | flops | bytes accessed | tf_op | source)
XLA Modules:
  0.0 164.1 jit_solution(15969078561055886669)
XLA Ops:
  7.2 1.1 fusion.19
  8.3 8.4 %psum.14 = f32[128]{0:T(128)S(1)} all-reduce(f32[128]{0:T(128)S(1)} %fusion.19), channel_id=1, replica_groups=mesh['kv'=8,'tp'=4] {'tp'}, use_global_device_ids=true, to_apply=%region_1.3 | all-reduce | flops 128 | bytes 1024 | tf_op jit(solution)/shard_map/psum | solution.py:82
  17.4 0.9 copy.75
  18.4 5.7 %fusion.16 = bf16[128,3088]{0,1:T(8,128)(2,1)S(1)} fusion(bf16[1024,16]{1,0:T(8,128)(2,1)S(1)} %copy.75, bf16[1024,1024]{1,0:T(8,128)(2,1)} %param.23, bf16[1024,1024]{1,0:T(8,128)(2,1)} %param.22, bf16[1024,1024]{1,0:T(8,128)(2,1)} %param.21, bf16[128,1024]{1,0:T(8,128)(2,1)} %param.19, f32[1024]{0:T(1024)S(1)} %convert_element_type.130, ...), kind=kOutput, calls=%fused_computation.20 | convolution fusion | flops 835717120 | bytes 7381504 | tf_op jit(solution)/shard_map/dot_general | solution.py:87
  24.1 1.7 %copy.94 = bf16[128,3088]{1,0:T(8,128)(2,1)} copy(bf16[128,3088]{0,1:T(8,128)(2,1)S(1)} %fusion.16) | data formatting | bytes 1581056
  26.4 0.9 gather_fusion.2
  27.3 0.9 gather_fusion.1
  28.2 10.2 %gather_fusion = f32[8,16,64,128]{3,2,1,0:T(8,128)} fusion(f32[8,5,16,64,128]{4,3,2,1,0:T(8,128)} %param.32, s32[8]{0:T(128)S(1)} %or_bitcast_fusion), kind=kCustom, calls=%fused_computation.2 | custom fusion | bytes 8388672 | tf_op jit(solution)/shard_map/jit(take_along_axis)/gather | solution.py:122
  38.6 5.2 %broadcast_select_fusion.1 = f32[8,16,64,128]{3,2,1,0:T(8,128)} fusion(f32[8,16,64,128]{3,2,1,0:T(8,128)} %gather_fusion, pred[8]{0:T(512)(128)(4,1)S(1)} %compare_and_fusion), kind=kLoop, calls=%fused_computation.21 | loop fusion | flops 1048576 | bytes 8388616 | tf_op jit(solution)/shard_map/jit(take_along_axis)/select_n | solution.py:122
  43.8 6.5 %broadcast_select_fusion = f32[8,1,16,64,128]{4,1,3,2,0:T(1,128)} fusion(f32[8,1,16,64,128]{4,1,3,2,0:T(1,128)S(1)} %bitcast.44, pred[8]{0:T(512)(128)(4,1)S(1)} %compare_and_fusion), kind=kLoop, calls=%fused_computation.11 | loop fusion | flops 1048576 | bytes 8388616 | tf_op jit(solution)/shard_map/jit(take_along_axis)/select_n | solution.py:122
  51.3 0.9 fusion.54
  52.5 0.7 copy.89
  53.2 0.7 copy.88
  55.1 2.9 %copy.82 = f32[8,4,16,64]{1,3,2,0:T(8,128)} copy(f32[8,4,16,64]{3,2,1,0:T(8,128)S(1)} %broadcast_multiply_fusion) | data formatting | bytes 262144 | tf_op jit(solution)/shard_map/mul | solution.py:46
  58.0 15.6 %bitcast_add_fusion = f32[8,4,16,64,128]{4,1,3,2,0:T(4,128)S(1)} fusion(f32[8,4,16,128]{3,1,2,0:T(4,128)S(1)} %bitcast.45, f32[8,4,16,64]{1,3,2,0:T(8,128)} %copy.82, f32[8,16,64,128]{3,2,1,0:T(8,128)} %broadcast_select_fusion.1, f32[8,4,16]{1,2,0:T(8,128)S(1)} %copy.78, f32[8,4,16]{1,2,0:T(8,128)S(1)} %copy.84, pred[4,4]{1,0:T(4,128)(4,1)S(1)} %iota_compare_fusion), kind=kOutput, calls=%fused_computation.4 | convolution fusion | flops 46141440 | bytes 21368848 | tf_op jit(solution)/shard_map/strh,srhpn->sthpn/dot_general | solution.py:48
  73.8 6.1 %copy-done.3 = f32[8,4,16,64,128]{4,1,3,2,0:T(4,128)} copy-done((f32[8,4,16,64,128]{4,1,3,2,0:T(4,128)}, f32[8,4,16,64,128]{4,1,3,2,0:T(4,128)S(1)}, u32[]{:S(2)}) %copy-start.3) | copy-done | bytes 16777240
  79.8 5.1 %fusion = f32[8,4,16,1,64]{4,3,2,1,0:T(1,128)} fusion(f32[8,4,16,128,1]{3,4,2,1,0:T(1,128)S(1)} %bitcast.46, f32[8,4,16,64,128]{4,1,3,2,0:T(4,128)S(1)} %bitcast_add_fusion), kind=kOutput, calls=%fused_computation.5 | convolution fusion | flops 8388608 | bytes 17170432 | tf_op jit(solution)/shard_map/sthn,sthpn->sthp/dot_general | solution.py:51
  85.0 1.2 multiply_reduce_fusion
  86.4 5.7 %fusion.33 = f32[32,4096]{1,0:T(8,128)} fusion(bf16[1024,4096]{1,0:T(8,128)(2,1)} %param.31, f32[32,1024]{1,0:T(8,128)S(1)} %reshape.214, f32[1024]{0:T(1024)S(1)} %convert_element_type.157), kind=kOutput, calls=%fused_computation.57 | convolution fusion | flops 268500992 | bytes 9048064 | tf_op jit(solution)/shard_map/dot_general | solution.py:133
  92.2 20.0 %pad_maximum_fusion = f32[8,5,16,64,128]{4,1,3,2,0:T(8,128)} fusion(f32[8,4,16,64,128]{4,1,3,2,0:T(4,128)} %copy-done.3, f32[8,1,16,64,128]{4,1,3,2,0:T(1,128)} %broadcast_select_fusion), kind=kLoop, calls=%fused_computation.3 | loop fusion | flops 5242880 | bytes 41943040 | tf_op jit(solution)/shard_map/concatenate | solution.py:128
  112.2 19.5 %copy.87 = f32[8,5,16,64,128]{4,3,2,1,0:T(8,128)} copy(f32[8,5,16,64,128]{4,1,3,2,0:T(8,128)} %pad_maximum_fusion) | data formatting | bytes 41943040
  131.6 21.9 %psum.15 = f32[32]{0:T(128)S(1)} all-reduce(f32[32]{0:T(128)S(1)} %reduce_sum.22), channel_id=1, replica_groups=mesh['kv'=8,'tp'=4] {'kv'}, use_global_device_ids=true, to_apply=%region_5.7 | all-reduce | flops 32 | bytes 256 | tf_op jit(solution)/shard_map/psum | solution.py:134
  153.5 2.3 %reduce-scatter.5.cloned.1.call-done = f32[32,512]{1,0:T(8,128)} async-done(((f32[32,4096]{1,0:T(8,128)}), f32[32,512]{1,0:T(8,128)}) %reduce-scatter.5.cloned.1.call-update) | async-done | bytes 65552 | tf_op jit(solution)/shard_map/reduce_scatter | solution.py:135
  155.8 1.5 multiply_convert_fusion.2
  (69 shorter events, 4.1 us)
Async XLA Ops:
  7.2 19.2 %copy-start = (bf16[8,7,1024]{2,0,1:T(8,128)(2,1)S(1)}, bf16[8,7,1024]{2,0,1:T(8,128)(2,1)}, u32[]{:S(2)}) copy-start(bf16[8,7,1024]{2,0,1:T(8,128)(2,1)} %param.33) | copy-start | bytes 344068
  7.2 43.1 %reduce-scatter.7.cloned.1.call-start = ((), (), s32[]{:S(2)}) async-start(), calls=%async_computation.3 | async-start | bytes 1024000 | tf_op jit(solution)/shard_map/reduce_scatter | solution.py:88
  18.3 7.6 %copy-start.10 = (s32[8]{0:T(128)S(1)}, s32[8]{0:T(128)}, u32[]{:S(2)}) copy-start(s32[8]{0:T(128)} %param.35) | copy-start | bytes 100
  18.3 7.6 %copy-start.11 = (f32[16]{0:T(128)S(1)}, f32[16]{0:T(128)}, u32[]{:S(2)}) copy-start(f32[16]{0:T(128)} %param.28) | copy-start | bytes 196
  18.3 7.7 %copy-start.5 = (bf16[4,1024]{1,0:T(4,128)(2,1)S(1)}, bf16[4,1024]{1,0:T(4,128)(2,1)}, u32[]{:S(2)}) copy-start(bf16[4,1024]{1,0:T(4,128)(2,1)} %param.25) | copy-start | bytes 24580
  18.4 7.7 %copy-start.6 = (bf16[4,1024]{1,0:T(4,128)(2,1)S(1)}, bf16[4,1024]{1,0:T(4,128)(2,1)}, u32[]{:S(2)}) copy-start(bf16[4,1024]{1,0:T(4,128)(2,1)} %param.26) | copy-start | bytes 24580
  18.4 8.0 %copy-start.7 = (bf16[1024]{0:T(1024)(128)(2,1)S(1)}, bf16[1024]{0:T(1024)(128)(2,1)}, u32[]{:S(2)}) copy-start(bf16[1024]{0:T(1024)(128)(2,1)} %param.30) | copy-start | bytes 6148
  18.4 8.9 %copy-start.4 = (bf16[8,7,1024]{2,0,1:T(8,128)(2,1)S(1)}, bf16[8,7,1024]{2,0,1:T(8,128)(2,1)}, u32[]{:S(2)}) copy-start(bf16[8,7,1024]{2,0,1:T(8,128)(2,1)} %param.34) | copy-start | bytes 344068
  25.8 130.0 %reduce-scatter.5.cloned.1.call-start = ((), (), s32[]{:S(2)}) async-start(), calls=%async_computation.2 | async-start | bytes 589824 | tf_op jit(solution)/shard_map/reduce_scatter | solution.py:135
  38.4 5.3 %copy-start.2 = (f32[8,16,64,128]{3,2,1,0:T(8,128)S(1)}, f32[8,16,64,128]{3,2,1,0:T(8,128)}, u32[]{:S(2)}) copy-start(f32[8,16,64,128]{3,2,1,0:T(8,128)} %gather_fusion) | copy-start | bytes 12582916
  38.6 12.4 %copy-start.8 = (f32[16]{0:T(128)S(1)}, f32[16]{0:T(128)}, u32[]{:S(2)}) copy-start(f32[16]{0:T(128)} %param.27) | copy-start | bytes 196
  73.7 6.2 %copy-start.3 = (f32[8,4,16,64,128]{4,1,3,2,0:T(4,128)}, f32[8,4,16,64,128]{4,1,3,2,0:T(4,128)S(1)}, u32[]{:S(2)}) copy-start(f32[8,4,16,64,128]{4,1,3,2,0:T(4,128)S(1)} %bitcast_add_fusion) | copy-start | bytes 50331652
  73.7 11.3 %copy-start.9 = (f32[16]{0:T(128)S(1)}, f32[16]{0:T(128)}, u32[]{:S(2)}) copy-start(f32[16]{0:T(128)} %param.29) | copy-start | bytes 196
  112.2 45.1 %copy-start.1 = (bf16[8,7,1024]{2,0,1:T(8,128)(2,1)S(1)}, bf16[8,7,1024]{2,0,1:T(8,128)(2,1)}, u32[]{:S(2)}) copy-start(bf16[8,7,1024]{2,0,1:T(8,128)(2,1)} %param.33) | copy-start | bytes 344068
Sparse Core Ops, SparseCore 0:
  25.9 23.7 reduce-scatter.6
  92.3 63.4 reduce-scatter.4
where the time goes:
time: 165 us; the launch traced here: 164 us
  local copies, waits for them, and re-layouts  46.8 us (28%)
  other arithmetic  38.2 us (23%)
  matrix products  32.2 us (20%)
  blocking collectives  30.2 us (18%)
  between operations  14.4 us (9%)
  waiting for transfers between devices  2.31 us (1%)
    unnamed x30, local copies, waits for them, and re-layouts  29.7 us
    psum x1, blocking collectives, local(): total_squares = lax.psum(square_sum, 'kv')  21.9 us
    concatenate x1, other arithmetic, local(): new_states = jnp.concatenate([first_state[:, None], states], axis=1)  20 us
    dot_general x1, matrix products, ssd_block(): jnp.einsum('strh,srhpn->sthpn', weights, outer_prod)  15.6 us
    select_n x2, other arithmetic, local(): jnp.take_along_axis(saved_states, accepted[:, None, None, None, None], ax...  11.7 us
    gather x1, local copies, waits for them, and re-layouts, local(): jnp.take_along_axis(saved_states, accepted[:, None, None, None, None], ax...  10.2 us
    psum x1, blocking collectives, local(): squares = lax.psum(jnp.sum(widened * widened, axis=1), 'tp')  8.36 us
    dot_general x1, matrix products, local(): jnp.dot(scaled, output_weight, preferred_element_type=jnp.float32)  5.75 us
  transfers between devices with their start and end apart: 2, of which 1 were waited for; matrix products, arithmetic and copies ran while one was open for 39% of the time, Pallas kernels for 0%

commit v1 on v0

--- a/solution.py
+++ b/solution.py
@@ -79,7 +79,9 @@
     inner_here = x_weight.shape[1]
     bc_here = bc_weight.shape[1]
     widened = hidden.astype(jnp.float32)
-    squares = lax.psum(jnp.sum(widened * widened, axis=1), "tp")
+    x = jnp.sum(widened * widened, axis=1)
+    parts = lax.all_gather(x, "tp")
+    squares = jnp.sum(parts, axis=0)
     normed = (
         widened * lax.rsqrt(squares[:, None] / D + EPSILON) * input_gain.astype(jnp.float32)
     ).astype(jnp.bfloat16)

time: 165 us -> 164 us (level)
  blocking collectives: 30.2 us -> 27.4 us
  waiting for transfers between devices: 2.31 us -> 4.43 us
    psum x1 -> x0, blocking collectives: 8.36 us -> none  [local(): squares = lax.psum(jnp.sum(widened * widened, axis=1), 'tp')]
    all_gather x0 -> x1, blocking collectives: none -> 6 us  [local(): parts = lax.all_gather(x, 'tp')]
  transfers between devices with their start and end apart: 2 -> 2, of which waited for: 1 -> 2; matrix products, arithmetic and copies ran while one was open for 39% -> 39% of each run, Pallas kernels for 0% -> 0%
where the time goes in v1:
time: 164 us; the launch traced here: 163 us
  local copies, waits for them, and re-layouts  46.6 us (28%)
  other arithmetic  38.2 us (23%)
  matrix products  32.2 us (20%)
  blocking collectives  27.4 us (17%)
  between operations  14.4 us (9%)
  waiting for transfers between devices  4.43 us (3%)
    unnamed x30, local copies, waits for them, and re-layouts  29.7 us
    psum x1, blocking collectives, local(): total_squares = lax.psum(square_sum, 'kv')  21.4 us
    concatenate x1, other arithmetic, local(): new_states = jnp.concatenate([first_state[:, None], states], axis=1)  20 us
    dot_general x1, matrix products, ssd_block(): jnp.einsum('strh,srhpn->sthpn', weights, outer_prod)  15.6 us
    select_n x2, other arithmetic, local(): jnp.take_along_axis(saved_states, accepted[:, None, None, None, None], ax...  11.7 us
    gather x1, local copies, waits for them, and re-layouts, local(): jnp.take_along_axis(saved_states, accepted[:, None, None, None, None], ax...  10.1 us
    all_gather x1, blocking collectives, local(): parts = lax.all_gather(x, 'tp')  6 us
    dot_general x1, matrix products, local(): jnp.dot(scaled, output_weight, preferred_element_type=jnp.float32)  5.75 us
  transfers between devices with their start and end apart: 2, of which 2 were waited for; matrix products, arithmetic and copies ran while one was open for 39% of the time, Pallas kernels for 0%

profile of v1, /device:TPU:0, one launch (start us, length us, event | category | flops | bytes accessed | tf_op | source)
XLA Modules:
  0.0 163.3 jit_solution(3840665118973975195)
XLA Ops:
  7.2 1.1 fusion.19
  8.3 6.0 %all-gather.1 = f32[4,1,128]{2,1,0:T(1,128)S(1)} all-gather(f32[1,1,128]{2,1,0:T(1,128)S(1)} %bitcast.60), channel_id=2, replica_groups=mesh['kv'=8,'tp'=4] {'tp'}, dimensions={0}, use_global_device_ids=true | all-gather | bytes 2560 | tf_op jit(solution)/shard_map/all_gather | solution.py:83
  15.0 0.9 copy.75
  16.1 5.7 %fusion.16 = bf16[128,3088]{0,1:T(8,128)(2,1)S(1)} fusion(bf16[1024,16]{1,0:T(8,128)(2,1)S(1)} %copy.75, bf16[1024,1024]{1,0:T(8,128)(2,1)} %param.23, bf16[1024,1024]{1,0:T(8,128)(2,1)} %param.22, bf16[1024,1024]{1,0:T(8,128)(2,1)} %param.21, bf16[128,1024]{1,0:T(8,128)(2,1)} %param.19, f32[1024]{0:T(1024)S(1)} %convert_element_type.130, ...), kind=kOutput, calls=%fused_computation.20 | convolution fusion | flops 835717120 | bytes 7381504 | tf_op jit(solution)/shard_map/dot_general | solution.py:89
  21.7 1.7 %copy.94 = bf16[128,3088]{1,0:T(8,128)(2,1)} copy(bf16[128,3088]{0,1:T(8,128)(2,1)S(1)} %fusion.16) | data formatting | bytes 1581056
  24.0 0.9 gather_fusion.2
  25.0 0.9 gather_fusion.1
  25.9 10.1 %gather_fusion = f32[8,16,64,128]{3,2,1,0:T(8,128)} fusion(f32[8,5,16,64,128]{4,3,2,1,0:T(8,128)} %param.32, s32[8]{0:T(128)S(1)} %or_bitcast_fusion), kind=kCustom, calls=%fused_computation.2 | custom fusion | bytes 8388672 | tf_op jit(solution)/shard_map/jit(take_along_axis)/gather | solution.py:124
  36.1 5.2 %broadcast_select_fusion.1 = f32[8,16,64,128]{3,2,1,0:T(8,128)} fusion(f32[8,16,64,128]{3,2,1,0:T(8,128)} %gather_fusion, pred[8]{0:T(512)(128)(4,1)S(1)} %compare_and_fusion), kind=kLoop, calls=%fused_computation.21 | loop fusion | flops 1048576 | bytes 8388616 | tf_op jit(solution)/shard_map/jit(take_along_axis)/select_n | solution.py:124
  41.3 6.5 %broadcast_select_fusion = f32[8,1,16,64,128]{4,1,3,2,0:T(1,128)} fusion(f32[8,1,16,64,128]{4,1,3,2,0:T(1,128)S(1)} %bitcast.45, pred[8]{0:T(512)(128)(4,1)S(1)} %compare_and_fusion), kind=kLoop, calls=%fused_computation.11 | loop fusion | flops 1048576 | bytes 8388616 | tf_op jit(solution)/shard_map/jit(take_along_axis)/select_n | solution.py:124
  47.8 1.1 reduce-scatter.7.cloned.1.call-done
  49.9 0.9 fusion.54
  51.0 0.7 copy.89
  53.7 2.9 %copy.82 = f32[8,4,16,64]{1,3,2,0:T(8,128)} copy(f32[8,4,16,64]{3,2,1,0:T(8,128)S(1)} %broadcast_multiply_fusion) | data formatting | bytes 262144 | tf_op jit(solution)/shard_map/mul | solution.py:46
  56.6 15.6 %bitcast_add_fusion = f32[8,4,16,64,128]{4,1,3,2,0:T(4,128)S(1)} fusion(f32[8,4,16,128]{3,1,2,0:T(4,128)S(1)} %bitcast.46, f32[8,4,16,64]{1,3,2,0:T(8,128)} %copy.82, f32[8,16,64,128]{3,2,1,0:T(8,128)} %broadcast_select_fusion.1, f32[8,4,16]{1,2,0:T(8,128)S(1)} %copy.78, f32[8,4,16]{1,2,0:T(8,128)S(1)} %copy.84, pred[4,4]{1,0:T(4,128)(4,1)S(1)} %iota_compare_fusion), kind=kOutput, calls=%fused_computation.4 | convolution fusion | flops 46141440 | bytes 21368848 | tf_op jit(solution)/shard_map/strh,srhpn->sthpn/dot_general | solution.py:48
  72.3 6.1 %copy-done.3 = f32[8,4,16,64,128]{4,1,3,2,0:T(4,128)} copy-done((f32[8,4,16,64,128]{4,1,3,2,0:T(4,128)}, f32[8,4,16,64,128]{4,1,3,2,0:T(4,128)S(1)}, u32[]{:S(2)}) %copy-start.3) | copy-done | bytes 16777240
  78.4 5.1 %fusion = f32[8,4,16,1,64]{4,3,2,1,0:T(1,128)} fusion(f32[8,4,16,128,1]{3,4,2,1,0:T(1,128)S(1)} %bitcast.47, f32[8,4,16,64,128]{4,1,3,2,0:T(4,128)S(1)} %bitcast_add_fusion), kind=kOutput, calls=%fused_computation.5 | convolution fusion | flops 8388608 | bytes 17170432 | tf_op jit(solution)/shard_map/sthn,sthpn->sthp/dot_general | solution.py:51
  83.5 1.2 multiply_reduce_fusion
  85.0 5.7 %fusion.33 = f32[32,4096]{1,0:T(8,128)} fusion(bf16[1024,4096]{1,0:T(8,128)(2,1)} %param.31, f32[32,1024]{1,0:T(8,128)S(1)} %reshape.218, f32[1024]{0:T(1024)S(1)} %convert_element_type.157), kind=kOutput, calls=%fused_computation.57 | convolution fusion | flops 268500992 | bytes 9048064 | tf_op jit(solution)/shard_map/dot_general | solution.py:135
  90.7 20.0 %pad_maximum_fusion = f32[8,5,16,64,128]{4,1,3,2,0:T(8,128)} fusion(f32[8,4,16,64,128]{4,1,3,2,0:T(4,128)} %copy-done.3, f32[8,1,16,64,128]{4,1,3,2,0:T(1,128)} %broadcast_select_fusion), kind=kLoop, calls=%fused_computation.3 | loop fusion | flops 5242880 | bytes 41943040 | tf_op jit(solution)/shard_map/concatenate | solution.py:130
  110.7 19.5 %copy.87 = f32[8,5,16,64,128]{4,3,2,1,0:T(8,128)} copy(f32[8,5,16,64,128]{4,1,3,2,0:T(8,128)} %pad_maximum_fusion) | data formatting | bytes 41943040
  130.2 21.4 %psum.7 = f32[32]{0:T(128)S(1)} all-reduce(f32[32]{0:T(128)S(1)} %reduce_sum.32), channel_id=1, replica_groups=mesh['kv'=8,'tp'=4] {'kv'}, use_global_device_ids=true, to_apply=%region_5.7 | all-reduce | flops 32 | bytes 256 | tf_op jit(solution)/shard_map/psum | solution.py:136
  151.6 3.3 %reduce-scatter.5.cloned.1.call-done = f32[32,512]{1,0:T(8,128)} async-done(((f32[32,4096]{1,0:T(8,128)}), f32[32,512]{1,0:T(8,128)}) %reduce-scatter.5.cloned.1.call-update) | async-done | bytes 65552 | tf_op jit(solution)/shard_map/reduce_scatter | solution.py:137
  154.9 1.5 multiply_convert_fusion.2
  (70 shorter events, 4.9 us)
Async XLA Ops:
  7.2 16.8 %copy-start = (bf16[8,7,1024]{2,0,1:T(8,128)(2,1)S(1)}, bf16[8,7,1024]{2,0,1:T(8,128)(2,1)}, u32[]{:S(2)}) copy-start(bf16[8,7,1024]{2,0,1:T(8,128)(2,1)} %param.33) | copy-start | bytes 344068
  7.2 41.7 %reduce-scatter.7.cloned.1.call-start = ((), (), s32[]{:S(2)}) async-start(), calls=%async_computation.3 | async-start | bytes 1024000 | tf_op jit(solution)/shard_map/reduce_scatter | solution.py:90
  16.0 7.6 %copy-start.10 = (s32[8]{0:T(128)S(1)}, s32[8]{0:T(128)}, u32[]{:S(2)}) copy-start(s32[8]{0:T(128)} %param.35) | copy-start | bytes 100
  16.0 7.6 %copy-start.11 = (f32[16]{0:T(128)S(1)}, f32[16]{0:T(128)}, u32[]{:S(2)}) copy-start(f32[16]{0:T(128)} %param.28) | copy-start | bytes 196
  16.0 7.7 %copy-start.5 = (bf16[4,1024]{1,0:T(4,128)(2,1)S(1)}, bf16[4,1024]{1,0:T(4,128)(2,1)}, u32[]{:S(2)}) copy-start(bf16[4,1024]{1,0:T(4,128)(2,1)} %param.25) | copy-start | bytes 24580
  16.0 7.7 %copy-start.6 = (bf16[4,1024]{1,0:T(4,128)(2,1)S(1)}, bf16[4,1024]{1,0:T(4,128)(2,1)}, u32[]{:S(2)}) copy-start(bf16[4,1024]{1,0:T(4,128)(2,1)} %param.26) | copy-start | bytes 24580
  16.0 8.0 %copy-start.7 = (bf16[1024]{0:T(1024)(128)(2,1)S(1)}, bf16[1024]{0:T(1024)(128)(2,1)}, u32[]{:S(2)}) copy-start(bf16[1024]{0:T(1024)(128)(2,1)} %param.30) | copy-start | bytes 6148
  16.0 8.9 %copy-start.4 = (bf16[8,7,1024]{2,0,1:T(8,128)(2,1)S(1)}, bf16[8,7,1024]{2,0,1:T(8,128)(2,1)}, u32[]{:S(2)}) copy-start(bf16[8,7,1024]{2,0,1:T(8,128)(2,1)} %param.34) | copy-start | bytes 344068
  23.5 131.4 %reduce-scatter.5.cloned.1.call-start = ((), (), s32[]{:S(2)}) async-start(), calls=%async_computation.2 | async-start | bytes 589824 | tf_op jit(solution)/shard_map/reduce_scatter | solution.py:137
  35.9 5.3 %copy-start.2 = (f32[8,16,64,128]{3,2,1,0:T(8,128)S(1)}, f32[8,16,64,128]{3,2,1,0:T(8,128)}, u32[]{:S(2)}) copy-start(f32[8,16,64,128]{3,2,1,0:T(8,128)} %gather_fusion) | copy-start | bytes 12582916
  36.1 13.5 %copy-start.8 = (f32[16]{0:T(128)S(1)}, f32[16]{0:T(128)}, u32[]{:S(2)}) copy-start(f32[16]{0:T(128)} %param.27) | copy-start | bytes 196
  72.2 6.2 %copy-start.3 = (f32[8,4,16,64,128]{4,1,3,2,0:T(4,128)}, f32[8,4,16,64,128]{4,1,3,2,0:T(4,128)S(1)}, u32[]{:S(2)}) copy-start(f32[8,4,16,64,128]{4,1,3,2,0:T(4,128)S(1)} %bitcast_add_fusion) | copy-start | bytes 50331652
  72.3 11.3 %copy-start.9 = (f32[16]{0:T(128)S(1)}, f32[16]{0:T(128)}, u32[]{:S(2)}) copy-start(f32[16]{0:T(128)} %param.29) | copy-start | bytes 196
  110.7 45.7 %copy-start.1 = (bf16[8,7,1024]{2,0,1:T(8,128)(2,1)S(1)}, bf16[8,7,1024]{2,0,1:T(8,128)(2,1)}, u32[]{:S(2)}) copy-start(bf16[8,7,1024]{2,0,1:T(8,128)(2,1)} %param.33) | copy-start | bytes 344068
Sparse Core Ops, SparseCore 0:
  23.6 25.1 reduce-scatter.6
  90.8 63.9 reduce-scatter.4
